TPU v7x, 512 devices: a whole 4x4x16 slice. The times are simulated.
512 devices in a mesh: sp: 128 (over z, x, core), tp: 4 (over y).
Axes of the slice: x: 4, y: 4, z: 16, core: 2. Of those that a mesh axis runs over, the one named last changes fastest.
Arguments:
- tokens: bfloat16 [32768, 2048], P(('sp', 'tp')), may hold values from -40 to 40
- w_query: bfloat16 [2048, 1024], P(None, 'tp'), may hold values from -0.125 to 0.125
- w_key: bfloat16 [2048, 256], P(None, 'tp'), may hold values from -0.125 to 0.125
- w_value: bfloat16 [2048, 256], P(None, 'tp'), may hold values from -0.125 to 0.125
- w_out: bfloat16 [1024, 2048], P('tp'), may hold values from -0.1875 to 0.1875
- cum_gate: float32 [16, 32768], P('tp', 'sp'), may hold values from -4684 to 0, as said below
Outputs:
- layer_out: bfloat16 [32768, 2048], P(('sp', 'tp'))
Inputs may be any that keep to these rules, and one draw needn't show every extreme that they name: `cum_gate`: each head's row does not rise along the positions.
All inputs are finite; a program needn't handle non-finite values.
Results may differ from a plain program's by a relative error of at most 0.012.
Values may be sent and summed in bfloat16 or wider, within the bound.
No kernel may reach another device: no remote copies, remote signals or barrier semaphores. Data moves between devices by JAX's collectives and lax.ppermute only.
A program may use at most 64 MiB of HBM per device.

v0:
```python
import math
import jax
import jax.numpy as jnp
from jax import lax
from jax.sharding import PartitionSpec as P

HD = 64


def sent_to_all(x, axis):
    copies = jnp.broadcast_to(x, (lax.axis_size(axis), *x.shape))
    return lax.all_to_all(copies, axis, split_axis=0, concat_axis=0, tiled=True)


def joined_along(parts, dim):
    dims = list(parts.shape[1:])
    dims[dim] *= parts.shape[0]
    return jnp.moveaxis(parts, 0, dim).reshape(dims)


def collect(x, axis, dim):
    parts = sent_to_all(x, axis)
    return joined_along(parts, dim)


def partner(block, axis, bit):
    count = lax.axis_size(axis)
    route = []
    for low in range(count):
        high = low | 1 << bit
        if high != low and high < count:
            route += [(low, high), (high, low)]
    return lax.ppermute(block, axis, route)


def cut_along(x, dim, peers):
    before, after = (x.shape[:dim], x.shape[dim + 1 :])
    return jnp.moveaxis(x.reshape(*before, peers, -1, *after), dim, 0)


def sent_and_summed(x, axis, dim):
    peers = lax.axis_size(axis)
    parts = lax.all_to_all(cut_along(x, dim, peers), axis, 0, 0, tiled=True)
    return jnp.sum(parts.astype(jnp.float32), axis=0)


def per_device(tokens, w_query, w_key, w_value, w_out, cum_gate):
    pieces = collect(tokens, "tp", 0)
    query_part = jnp.dot(pieces, w_query, preferred_element_type=jnp.float32).astype(jnp.bfloat16)
    key_part = jnp.dot(pieces, w_key, preferred_element_type=jnp.float32).astype(jnp.bfloat16)
    value_part = jnp.dot(pieces, w_value, preferred_element_type=jnp.float32).astype(jnp.bfloat16)
    projected = jnp.concatenate([query_part, key_part, value_part], axis=1)
    row_count = projected.shape[0]
    half_rows = row_count // 2
    heads_local = w_query.shape[1] // HD
    kv_local = w_key.shape[1] // HD
    group_size = heads_local // kv_local
    score_factor = float(HD) ** (-0.5)
    query_flat = projected[:, : heads_local * HD]
    key_values = projected[:, heads_local * HD :]
    first_pos = lax.axis_index("sp") * row_count
    own_pos = first_pos + jnp.arange(row_count, dtype=jnp.int32)
    gate_all = lax.all_gather(cum_gate, "sp", axis=1, tiled=True)
    partner_leading = (lax.axis_size("sp") - 1 - lax.axis_index("sp")) * row_count
    moved = query_flat[half_rows:]
    for bit in range(lax.axis_size("sp").bit_length() - 1):
        moved = partner(moved, "sp", bit)
    partner_start = partner_leading + half_rows
    partner_pos = partner_start + jnp.arange(half_rows, dtype=jnp.int32)
    partner_cum = lax.dynamic_slice_in_dim(gate_all, partner_start, half_rows, 1)
    groups = [
        (query_flat[:half_rows], cum_gate[:, :half_rows], own_pos[:half_rows]),
        (moved, partner_cum, partner_pos),
    ]
    prepared = []
    for query_rows, query_gates, query_pos in groups:
        count = query_rows.shape[0]
        prepared.append(
            (
                query_rows.reshape(count, kv_local, group_size, HD),
                query_gates.reshape(kv_local, group_size, count, 1),
                query_pos,
                jnp.max(query_pos),
            )
        )
    initial = tuple(
        (
            (
                jnp.full((kv_local, group_size, member[2].shape[0]), -1e30, jnp.float32),
                jnp.zeros((kv_local, group_size, member[2].shape[0]), jnp.float32),
                jnp.zeros((kv_local, group_size, member[2].shape[0], HD), jnp.float32),
            )
            for member in prepared
        )
    )
    pieces = lax.all_gather(key_values, "sp", axis=0, tiled=True)
    piece_rows = pieces.shape[0]
    key_block = math.gcd(piece_rows, 1024)

    def one_block(index, hidden_vectors):
        block_start = index * key_block
        slab = lax.dynamic_slice_in_dim(pieces, block_start, key_block, 0)
        key_rows = slab[:, : kv_local * HD].reshape(key_block, kv_local, HD)
        value_rows = slab[:, kv_local * HD :].reshape(key_block, kv_local, HD)
        key_cum = lax.dynamic_slice_in_dim(gate_all, block_start, key_block, 1)
        key_cum = key_cum.reshape(kv_local, group_size, 1, key_block)
        key_pos = block_start + jnp.arange(key_block, dtype=jnp.int32)
        results = []
        for member, state in zip(prepared, hidden_vectors):
            queries, query_cum, query_pos, last_pos = member

            def compute(inner, queries=queries, query_cum=query_cum, query_pos=query_pos):
                top_score, weight_sum, accumulated = inner
                scores = (
                    jnp.einsum(
                        "tkgd,skd->kgts", queries, key_rows, preferred_element_type=jnp.float32
                    )
                    * score_factor
                )
                scores = scores + (query_cum - key_cum)
                scores = jnp.where(key_pos[None, :] <= query_pos[:, None], scores, -jnp.inf)
                new_top = jnp.maximum(top_score, jnp.max(scores, axis=-1))
                weights = jnp.exp(scores - new_top[..., None])
                decay = jnp.exp(top_score - new_top)
                weight_sum = weight_sum * decay + jnp.sum(weights, axis=-1)
                update = jnp.einsum(
                    "kgts,skd->kgtd",
                    weights.astype(jnp.bfloat16),
                    value_rows,
                    preferred_element_type=jnp.float32,
                )
                accumulated = accumulated * decay[..., None] + update
                return (new_top, weight_sum, accumulated)

            def skipped(inner):
                return inner

            results.append(lax.cond(block_start <= last_pos, compute, skipped, state))
        return tuple(results)

    finals = lax.fori_loop(0, piece_rows // key_block, one_block, initial)
    parts = []
    for top_score, weight_sum, accumulated in finals:
        count = weight_sum.shape[2]
        rows = (accumulated / weight_sum[..., None]).astype(jnp.bfloat16)
        parts.append(rows.transpose(2, 0, 1, 3).reshape(count, heads_local * HD))
    attended = jnp.concatenate(parts, axis=0)
    returned = attended[half_rows:]
    for bit in range(lax.axis_size("sp").bit_length() - 1):
        returned = partner(returned, "sp", bit)
    attended = jnp.concatenate([attended[:half_rows], returned], axis=0)
    summed = sent_and_summed(
        jnp.dot(attended, w_out, preferred_element_type=jnp.float32).astype(jnp.bfloat16), "tp", 0
    )
    return summed.astype(jnp.bfloat16)


def solution(mesh):
    placed = (
        P(("sp", "tp"), None),
        P(None, "tp"),
        P(None, "tp"),
        P(None, "tp"),
        P("tp", None),
        P("tp", "sp"),
    )
    return jax.shard_map(
        per_device, mesh=mesh, in_specs=placed, out_specs=P(("sp", "tp"), None), check_vma=False
    )
```

profile of v0, /device:TPU:8, one launch (start us, length us, event | category | flops | bytes accessed | tf_op | source)
XLA Modules:
  0.0 399.6 jit_solution(4949304807565663179)
XLA Ops:
  7.7 18.5 %all_to_all.10 = bf16[4,64,2048]{2,1,0:T(8,128)(2,1)S(1)} all-to-all(bf16[4,64,2048]{2,1,0:T(8,128)(2,1)S(1)} %broadcast_in_dim.27), channel_id=1, replica_groups=mesh['sp'=128,'tp'=4] {'tp'}, dimensions={0} | all-to-all | bytes 2097152 | tf_op jit(solution)/shard_map/all_to_all | solution.py:12
  28.4 1.9 collective-permute-start
  31.5 3.4 collective-permute-start.1
  34.9 2.7 collective-permute-done.1
  37.7 4.9 %collective-permute-start.2 = (bf16[128,256]{0,1:T(8,128)(2,1)S(1)}, bf16[128,256]{0,1:T(8,128)(2,1)S(1)}, u32[]{:S(2)}, u32[]{:S(2)}) collective-permute-start(bf16[128,256]{0,1:T(8,128)(2,1)S(1)} %collective-permute-done.1), channel_id=1, source_target_pairs={{0,16},{16,0},{4,20},{20,4},{8,24},{24,8},{12,28},{28,12},{32,48},... | collective-permute-start | bytes 196616 | tf_op jit(solution)/shard_map/ppermute | solution.py:33
  42.6 2.7 collective-permute-done.2
  45.3 3.8 collective-permute-start.3
  49.1 2.3 collective-permute-done.3
  51.5 5.2 %collective-permute-start.4 = (bf16[128,256]{0,1:T(8,128)(2,1)S(1)}, bf16[128,256]{0,1:T(8,128)(2,1)S(1)}, u32[]{:S(2)}, u32[]{:S(2)}) collective-permute-start(bf16[128,256]{0,1:T(8,128)(2,1)S(1)} %collective-permute-done.3), channel_id=1, source_target_pairs={{0,64},{64,0},{4,68},{68,4},{8,72},{72,8},{12,76},{76,12},{16,80},... | collective-permute-start | bytes 196616 | tf_op jit(solution)/shard_map/ppermute | solution.py:33
  59.0 9.1 %collective-permute-start.5 = (bf16[128,256]{0,1:T(8,128)(2,1)S(1)}, bf16[128,256]{0,1:T(8,128)(2,1)S(1)}, u32[]{:S(2)}, u32[]{:S(2)}) collective-permute-start(bf16[128,256]{0,1:T(8,128)(2,1)S(1)} %collective-permute-done.4), channel_id=1, source_target_pairs={{0,128},{128,0},{4,132},{132,4},{8,136},{136,8},{12,140},{140,12},... | collective-permute-start | bytes 196616 | tf_op jit(solution)/shard_map/ppermute | solution.py:33
  68.1 86.7 %all_gather.7 = f32[4,32768]{1,0:T(4,128)S(1)} all-gather(f32[4,256]{1,0:T(4,128)S(1)} %copy-done.4), channel_id=1, replica_groups=mesh['sp'=128,'tp'=4] {'sp'}, dimensions={1}, use_global_device_ids=true | all-gather | bytes 528384 | tf_op jit(solution)/shard_map/all_gather | solution.py:63
  154.8 7.5 %collective-permute-start.6 = (bf16[128,256]{0,1:T(8,128)(2,1)S(1)}, bf16[128,256]{0,1:T(8,128)(2,1)S(1)}, u32[]{:S(2)}, u32[]{:S(2)}) collective-permute-start(bf16[128,256]{0,1:T(8,128)(2,1)S(1)} %collective-permute-done.5), channel_id=1, source_target_pairs={{0,256},{256,0},{4,260},{260,4},{8,264},{264,8},{12,268},{268,12},... | collective-permute-start | bytes 196616 | tf_op jit(solution)/shard_map/ppermute | solution.py:33
  162.3 13.1 %collective-permute-done.6 = bf16[128,256]{0,1:T(8,128)(2,1)S(1)} collective-permute-done((bf16[128,256]{0,1:T(8,128)(2,1)S(1)}, bf16[128,256]{0,1:T(8,128)(2,1)S(1)}, u32[]{:S(2)}, u32[]{:S(2)}) %collective-permute-start.6) | collective-permute-done | bytes 65568 | tf_op jit(solution)/shard_map/ppermute | solution.py:33
  175.4 9.9 %all-gather.2.cloned.1.call-done = bf16[32768,128]{0,1:T(8,128)(2,1)} async-done(((bf16[256,128]{0,1:T(8,128)(2,1)}), bf16[32768,128]{0,1:T(8,128)(2,1)}) %all-gather.2.cloned.1.call-update) | async-done | bytes 8388624 | tf_op jit(solution)/shard_map/all_gather | solution.py:96
  185.3 134.2 %while.24 = (s32[]{:T(128)}, f32[1,4,128]{2,1,0:T(4,128)S(1)}, f32[1,4,128]{2,1,0:T(4,128)S(1)}, f32[1,4,128,64]{2,3,1,0:T(8,128)S(1)}, f32[1,4,128]{2,1,0:T(4,1...) while((s32[]{:T(128)}, f32[1,4,128]{2,1,0:T(4,128)S(1)}, ...), condition=%wide.region_11.12_spmd.clone, body=%wide.region_2.11_spmd.clone.sunk | while | flops 278270080 | bytes 14961743 | solution.py:141
  197.7 1.8 conditional.7
  206.0 1.8 conditional.7
  214.3 1.8 conditional.7
  319.6 2.2 collective-permute-start.7
  322.7 1.9 collective-permute-start.8
  324.7 4.2 %collective-permute-done.8 = bf16[128,256]{0,1:T(8,128)(2,1)S(1)} collective-permute-done((bf16[128,256]{0,1:T(8,128)(2,1)S(1)}, bf16[128,256]{0,1:T(8,128)(2,1)S(1)}, u32[]{:S(2)}, u32[]{:S(2)}) %collective-permute-start.8) | collective-permute-done | bytes 65568 | tf_op jit(solution)/shard_map/ppermute | solution.py:33
  328.9 3.6 collective-permute-start.9
  332.5 4.1 %collective-permute-done.9 = bf16[128,256]{0,1:T(8,128)(2,1)S(1)} collective-permute-done((bf16[128,256]{0,1:T(8,128)(2,1)S(1)}, bf16[128,256]{0,1:T(8,128)(2,1)S(1)}, u32[]{:S(2)}, u32[]{:S(2)}) %collective-permute-start.9) | collective-permute-done | bytes 65568 | tf_op jit(solution)/shard_map/ppermute | solution.py:33
  336.5 4.2 %collective-permute-start.10 = (bf16[128,256]{0,1:T(8,128)(2,1)S(1)}, bf16[128,256]{0,1:T(8,128)(2,1)S(1)}, u32[]{:S(2)}, u32[]{:S(2)}) collective-permute-start(bf16[128,256]{0,1:T(8,128)(2,1)S(1)} %collective-permute-done.9), channel_id=1, source_target_pairs={{0,32},{32,0},{4,36},{36,4},{8,40},{40,8},{12,44},{44,12},{16,48},... | collective-permute-start | bytes 196616 | tf_op jit(solution)/shard_map/ppermute | solution.py:33
  340.7 2.2 collective-permute-done.10
  343.0 4.5 %collective-permute-start.11 = (bf16[128,256]{0,1:T(8,128)(2,1)S(1)}, bf16[128,256]{0,1:T(8,128)(2,1)S(1)}, u32[]{:S(2)}, u32[]{:S(2)}) collective-permute-start(bf16[128,256]{0,1:T(8,128)(2,1)S(1)} %collective-permute-done.10), channel_id=1, source_target_pairs={{0,64},{64,0},{4,68},{68,4},{8,72},{72,8},{12,76},{76,12},{16,80},... | collective-permute-start | bytes 196616 | tf_op jit(solution)/shard_map/ppermute | solution.py:33
  347.5 2.5 collective-permute-done.11
  350.0 6.7 %collective-permute-start.12 = (bf16[128,256]{0,1:T(8,128)(2,1)S(1)}, bf16[128,256]{0,1:T(8,128)(2,1)S(1)}, u32[]{:S(2)}, u32[]{:S(2)}) collective-permute-start(bf16[128,256]{0,1:T(8,128)(2,1)S(1)} %collective-permute-done.11), channel_id=1, source_target_pairs={{0,128},{128,0},{4,132},{132,4},{8,136},{136,8},{12,140},{140,12},... | collective-permute-start | bytes 196616 | tf_op jit(solution)/shard_map/ppermute | solution.py:33
  356.7 3.4 collective-permute-done.12
  360.1 8.7 %collective-permute-start.13 = (bf16[128,256]{0,1:T(8,128)(2,1)S(1)}, bf16[128,256]{0,1:T(8,128)(2,1)S(1)}, u32[]{:S(2)}, u32[]{:S(2)}) collective-permute-start(bf16[128,256]{0,1:T(8,128)(2,1)S(1)} %collective-permute-done.12), channel_id=1, source_target_pairs={{0,256},{256,0},{4,260},{260,4},{8,264},{264,8},{12,268},{268,12},... | collective-permute-start | bytes 196616 | tf_op jit(solution)/shard_map/ppermute | solution.py:33
  368.8 6.2 %collective-permute-done.13 = bf16[128,256]{0,1:T(8,128)(2,1)S(1)} collective-permute-done((bf16[128,256]{0,1:T(8,128)(2,1)S(1)}, bf16[128,256]{0,1:T(8,128)(2,1)S(1)}, u32[]{:S(2)}, u32[]{:S(2)}) %collective-permute-start.13) | collective-permute-done | bytes 65568 | tf_op jit(solution)/shard_map/ppermute | solution.py:33
  375.5 16.3 %all_to_all.11 = bf16[4,64,2048]{2,1,0:T(8,128)(2,1)S(1)} all-to-all(bf16[4,64,2048]{2,1,0:T(8,128)(2,1)S(1)} %bitcast.112), channel_id=1, replica_groups=mesh['sp'=128,'tp'=4] {'tp'}, dimensions={0} | all-to-all | bytes 2097152 | tf_op jit(solution)/shard_map/all_to_all | solution.py:43
  (489 shorter events, 153.8 us)
Async XLA Ops:
  6.5 368.5 %copy-start = (bf16[256,2048]{1,0:T(8,128)(2,1)S(1)}, bf16[256,2048]{1,0:T(8,128)(2,1)}, u32[]{:S(2)}) copy-start(bf16[256,2048]{1,0:T(8,128)(2,1)} %param.16) | copy-start | bytes 3145732
  6.5 19.7 %copy-start.2 = (bf16[2048,64]{0,1:T(8,128)(2,1)S(1)}, bf16[2048,64]{0,1:T(8,128)(2,1)}, u32[]{:S(2)}) copy-start(bf16[2048,64]{0,1:T(8,128)(2,1)} %param.15) | copy-start | bytes 786436
  6.5 178.7 %all-gather.2.cloned.1.call-start = ((), (), s32[]{:S(2)}) async-start(), calls=%async_computation.2 | async-start | bytes 8454144 | tf_op jit(solution)/shard_map/all_gather | solution.py:96
  6.5 20.1 %copy-start.3 = (bf16[2048,64]{0,1:T(8,128)(2,1)S(1)}, bf16[2048,64]{0,1:T(8,128)(2,1)}, u32[]{:S(2)}) copy-start(bf16[2048,64]{0,1:T(8,128)(2,1)} %param.14) | copy-start | bytes 786436
  7.7 20.1 %copy-start.1 = (bf16[2048,256]{1,0:T(8,128)(2,1)S(1)}, bf16[2048,256]{1,0:T(8,128)(2,1)}, u32[]{:S(2)}) copy-start(bf16[2048,256]{1,0:T(8,128)(2,1)} %param.13) | copy-start | bytes 3145732
  26.7 15.9 %copy-start.4 = (f32[4,256]{1,0:T(4,128)S(1)}, f32[4,256]{1,0:T(4,128)}, u32[]{:S(2)}) copy-start(f32[4,256]{1,0:T(4,128)} %param.17) | copy-start | bytes 12292
  28.4 3.1 collective-permute-start
  31.5 6.1 %collective-permute-start.1 = (bf16[128,256]{0,1:T(8,128)(2,1)S(1)}, bf16[128,256]{0,1:T(8,128)(2,1)S(1)}, u32[]{:S(2)}, u32[]{:S(2)}) collective-permute-start(bf16[128,256]{0,1:T(8,128)(2,1)S(1)} %collective-permute-done), channel_id=1, source_target_pairs={{0,8},{8,0},{4,12},{12,4},{16,24},{24,16},{20,28},{28,20},{32,40},... | collective-permute-start | bytes 196616 | tf_op jit(solution)/shard_map/ppermute | solution.py:33
  37.7 7.7 %collective-permute-start.2 = (bf16[128,256]{0,1:T(8,128)(2,1)S(1)}, bf16[128,256]{0,1:T(8,128)(2,1)S(1)}, u32[]{:S(2)}, u32[]{:S(2)}) collective-permute-start(bf16[128,256]{0,1:T(8,128)(2,1)S(1)} %collective-permute-done.1), channel_id=1, source_target_pairs={{0,16},{16,0},{4,20},{20,4},{8,24},{24,8},{12,28},{28,12},{32,48},... | collective-permute-start | bytes 196616 | tf_op jit(solution)/shard_map/ppermute | solution.py:33
  45.3 6.1 %collective-permute-start.3 = (bf16[128,256]{0,1:T(8,128)(2,1)S(1)}, bf16[128,256]{0,1:T(8,128)(2,1)S(1)}, u32[]{:S(2)}, u32[]{:S(2)}) collective-permute-start(bf16[128,256]{0,1:T(8,128)(2,1)S(1)} %collective-permute-done.2), channel_id=1, source_target_pairs={{0,32},{32,0},{4,36},{36,4},{8,40},{40,8},{12,44},{44,12},{16,48},... | collective-permute-start | bytes 196616 | tf_op jit(solution)/shard_map/ppermute | solution.py:33
  51.5 7.6 %collective-permute-start.4 = (bf16[128,256]{0,1:T(8,128)(2,1)S(1)}, bf16[128,256]{0,1:T(8,128)(2,1)S(1)}, u32[]{:S(2)}, u32[]{:S(2)}) collective-permute-start(bf16[128,256]{0,1:T(8,128)(2,1)S(1)} %collective-permute-done.3), channel_id=1, source_target_pairs={{0,64},{64,0},{4,68},{68,4},{8,72},{72,8},{12,76},{76,12},{16,80},... | collective-permute-start | bytes 196616 | tf_op jit(solution)/shard_map/ppermute | solution.py:33
  59.0 95.8 %collective-permute-start.5 = (bf16[128,256]{0,1:T(8,128)(2,1)S(1)}, bf16[128,256]{0,1:T(8,128)(2,1)S(1)}, u32[]{:S(2)}, u32[]{:S(2)}) collective-permute-start(bf16[128,256]{0,1:T(8,128)(2,1)S(1)} %collective-permute-done.4), channel_id=1, source_target_pairs={{0,128},{128,0},{4,132},{132,4},{8,136},{136,8},{12,140},{140,12},... | collective-permute-start | bytes 196616 | tf_op jit(solution)/shard_map/ppermute | solution.py:33
  154.8 20.5 %collective-permute-start.6 = (bf16[128,256]{0,1:T(8,128)(2,1)S(1)}, bf16[128,256]{0,1:T(8,128)(2,1)S(1)}, u32[]{:S(2)}, u32[]{:S(2)}) collective-permute-start(bf16[128,256]{0,1:T(8,128)(2,1)S(1)} %collective-permute-done.5), channel_id=1, source_target_pairs={{0,256},{256,0},{4,260},{260,4},{8,264},{264,8},{12,268},{268,12},... | collective-permute-start | bytes 196616 | tf_op jit(solution)/shard_map/ppermute | solution.py:33
  319.6 3.1 collective-permute-start.7
  322.7 6.1 %collective-permute-start.8 = (bf16[128,256]{0,1:T(8,128)(2,1)S(1)}, bf16[128,256]{0,1:T(8,128)(2,1)S(1)}, u32[]{:S(2)}, u32[]{:S(2)}) collective-permute-start(bf16[128,256]{0,1:T(8,128)(2,1)S(1)} %collective-permute-done.7), channel_id=1, source_target_pairs={{0,8},{8,0},{4,12},{12,4},{16,24},{24,16},{20,28},{28,20},{32,40},... | collective-permute-start | bytes 196616 | tf_op jit(solution)/shard_map/ppermute | solution.py:33
  328.9 7.7 %collective-permute-start.9 = (bf16[128,256]{0,1:T(8,128)(2,1)S(1)}, bf16[128,256]{0,1:T(8,128)(2,1)S(1)}, u32[]{:S(2)}, u32[]{:S(2)}) collective-permute-start(bf16[128,256]{0,1:T(8,128)(2,1)S(1)} %collective-permute-done.8), channel_id=1, source_target_pairs={{0,16},{16,0},{4,20},{20,4},{8,24},{24,8},{12,28},{28,12},{32,48},... | collective-permute-start | bytes 196616 | tf_op jit(solution)/shard_map/ppermute | solution.py:33
  336.5 6.4 %collective-permute-start.10 = (bf16[128,256]{0,1:T(8,128)(2,1)S(1)}, bf16[128,256]{0,1:T(8,128)(2,1)S(1)}, u32[]{:S(2)}, u32[]{:S(2)}) collective-permute-start(bf16[128,256]{0,1:T(8,128)(2,1)S(1)} %collective-permute-done.9), channel_id=1, source_target_pairs={{0,32},{32,0},{4,36},{36,4},{8,40},{40,8},{12,44},{44,12},{16,48},... | collective-permute-start | bytes 196616 | tf_op jit(solution)/shard_map/ppermute | solution.py:33
  343.0 7.0 %collective-permute-start.11 = (bf16[128,256]{0,1:T(8,128)(2,1)S(1)}, bf16[128,256]{0,1:T(8,128)(2,1)S(1)}, u32[]{:S(2)}, u32[]{:S(2)}) collective-permute-start(bf16[128,256]{0,1:T(8,128)(2,1)S(1)} %collective-permute-done.10), channel_id=1, source_target_pairs={{0,64},{64,0},{4,68},{68,4},{8,72},{72,8},{12,76},{76,12},{16,80},... | collective-permute-start | bytes 196616 | tf_op jit(solution)/shard_map/ppermute | solution.py:33
  350.0 10.1 %collective-permute-start.12 = (bf16[128,256]{0,1:T(8,128)(2,1)S(1)}, bf16[128,256]{0,1:T(8,128)(2,1)S(1)}, u32[]{:S(2)}, u32[]{:S(2)}) collective-permute-start(bf16[128,256]{0,1:T(8,128)(2,1)S(1)} %collective-permute-done.11), channel_id=1, source_target_pairs={{0,128},{128,0},{4,132},{132,4},{8,136},{136,8},{12,140},{140,12},... | collective-permute-start | bytes 196616 | tf_op jit(solution)/shard_map/ppermute | solution.py:33
  360.1 15.0 %collective-permute-start.13 = (bf16[128,256]{0,1:T(8,128)(2,1)S(1)}, bf16[128,256]{0,1:T(8,128)(2,1)S(1)}, u32[]{:S(2)}, u32[]{:S(2)}) collective-permute-start(bf16[128,256]{0,1:T(8,128)(2,1)S(1)} %collective-permute-done.12), channel_id=1, source_target_pairs={{0,256},{256,0},{4,260},{260,4},{8,264},{264,8},{12,268},{268,12},... | collective-permute-start | bytes 196616 | tf_op jit(solution)/shard_map/ppermute | solution.py:33
Sparse Core Ops, SparseCore 0:
  27.9 157.3 all-gather.1
where the time goes:
time: 401 us; the launch traced here: 400 us
  blocking collectives  121 us (30%)
  starting transfers between devices  67.5 us (17%)
  waiting for transfers between devices  56.7 us (14%)
  loops' own time  44.4 us (11%)
  matrix products  41.9 us (10%)
  local copies, waits for them, and re-layouts  33.5 us (8%)
  other arithmetic  20.3 us (5%)
  between operations  13.7 us (3%)
    all_gather x1, blocking collectives, per_device(): gate_all = lax.all_gather(cum_gate, 'sp', axis=1, tiled=True)  86.7 us
    ppermute x14, starting transfers between devices, partner(): return lax.ppermute(block, axis, route)  67.5 us
    ppermute x14, waiting for transfers between devices, partner(): return lax.ppermute(block, axis, route)  46.8 us
    another operation x1, loops' own time, per_device(): finals = lax.fori_loop(0, piece_rows // key_block, one_block, initial)  41.9 us
    reshape x32, local copies, waits for them, and re-layouts, one_block(): value_rows = slab[:, kv_local * HD:].reshape(key_block, kv_local, HD)  31.8 us
    dot_general x33, matrix products, compute(): jnp.einsum('tkgd,skd->kgts', queries, key_rows, preferred_element_type=jn...  24.4 us
    all_to_all x1, blocking collectives, sent_to_all(): return lax.all_to_all(copies, axis, split_axis=0, concat_axis=0, tiled=True)  18.5 us
    all_to_all x1, blocking collectives, sent_and_summed(): parts = lax.all_to_all(cut_along(x, dim, peers), axis, 0, 0, tiled=True)  16.3 us
  transfers between devices with their start and end apart: 15, of which 14 were waited for; matrix products, arithmetic and copies ran while one was open for 0% of the time, Pallas kernels for 0%

commit v1 on v0

--- a/solution.py
+++ b/solution.py
@@ -60,7 +60,10 @@
     key_values = projected[:, heads_local * HD :]
     first_pos = lax.axis_index("sp") * row_count
     own_pos = first_pos + jnp.arange(row_count, dtype=jnp.int32)
-    gate_all = lax.all_gather(cum_gate, "sp", axis=1, tiled=True)
+    size = lax.axis_size("sp")
+    blocks = jnp.stack([cum_gate for _ in range(size)])
+    blocks = lax.all_to_all(blocks, "sp", split_axis=0, concat_axis=0)
+    gate_all = jnp.concatenate(blocks, axis=1)
     partner_leading = (lax.axis_size("sp") - 1 - lax.axis_index("sp")) * row_count
     moved = query_flat[half_rows:]
     for bit in range(lax.axis_size("sp").bit_length() - 1):

time: 401 us -> 429 us (1.070)
  the two profiles are of different devices: /device:TPU:8 before, /device:TPU:64 now
where the time goes in v1:
time: 429 us; the launch traced here: 425 us
  waiting for transfers between devices  137 us (32%)
  starting transfers between devices  76.4 us (18%)
  local copies, waits for them, and re-layouts  58 us (14%)
  loops' own time  43.3 us (10%)
  matrix products  42 us (10%)
  blocking collectives  34.3 us (8%)
  other arithmetic  20.3 us (5%)
  between operations  13.7 us (3%)
    all_gather x1, waiting for transfers between devices, per_device(): pieces = lax.all_gather(key_values, 'sp', axis=0, tiled=True)  79.4 us
    ppermute x14, waiting for transfers between devices, partner(): return lax.ppermute(block, axis, route)  57.7 us
    ppermute x14, starting transfers between devices, partner(): return lax.ppermute(block, axis, route)  57.3 us
    another operation x1, loops' own time, per_device(): finals = lax.fori_loop(0, piece_rows // key_block, one_block, initial)  41.4 us
    reshape x32, local copies, waits for them, and re-layouts, one_block(): value_rows = slab[:, kv_local * HD:].reshape(key_block, kv_local, HD)  31.8 us
    dot_general x33, matrix products, compute(): jnp.einsum('tkgd,skd->kgts', queries, key_rows, preferred_element_type=jn...  24.5 us
    reshape x32, local copies, waits for them, and re-layouts, one_block(): key_cum = key_cum.reshape(kv_local, group_size, 1, key_block)  23.2 us
    all_to_all x1, blocking collectives, sent_to_all(): return lax.all_to_all(copies, axis, split_axis=0, concat_axis=0, tiled=True)  19.4 us
  transfers between devices with their start and end apart: 16, of which 15 were waited for; matrix products, arithmetic and copies ran while one was open for 1% of the time, Pallas kernels for 0%

profile of v1, /device:TPU:64, one launch (start us, length us, event | category | flops | bytes accessed | tf_op | source)
XLA Modules:
  0.0 425.2 jit_solution(13639488979500050847)
XLA Ops:
  7.7 19.4 %all_to_all.15 = bf16[4,64,2048]{2,1,0:T(8,128)(2,1)S(1)} all-to-all(bf16[4,64,2048]{2,1,0:T(8,128)(2,1)S(1)} %broadcast_in_dim.27), channel_id=1, replica_groups=mesh['sp'=128,'tp'=4] {'tp'}, dimensions={0} | all-to-all | bytes 2097152 | tf_op jit(solution)/shard_map/all_to_all | solution.py:12
  29.6 19.0 %all-to-all-start.1 = ((f32[128,4,256]{2,1,0:T(4,128)}), f32[128,4,256]{2,1,0:T(4,128)}, u32[]{:S(2)}, u32[]{:S(2)}) async-start(f32[128,4,256]{2,1,0:T(4,128)} %stack.2), calls=%async_computation.1 | async-start | bytes 1048576 | tf_op jit(solution)/shard_map/all_to_all | solution.py:65
  49.1 2.0 collective-permute-start
  52.3 3.4 collective-permute-start.1
  55.7 3.1 collective-permute-done.1
  58.7 5.2 %collective-permute-start.2 = (bf16[128,256]{0,1:T(8,128)(2,1)S(1)}, bf16[128,256]{0,1:T(8,128)(2,1)S(1)}, u32[]{:S(2)}, u32[]{:S(2)}) collective-permute-start(bf16[128,256]{0,1:T(8,128)(2,1)S(1)} %collective-permute-done.1), channel_id=1, source_target_pairs={{0,16},{16,0},{4,20},{20,4},{8,24},{24,8},{12,28},{28,12},{32,48},... | collective-permute-start | bytes 196616 | tf_op jit(solution)/shard_map/ppermute | solution.py:33
  63.9 2.6 collective-permute-done.2
  66.6 3.8 collective-permute-start.3
  70.4 4.3 %collective-permute-done.3 = bf16[128,256]{0,1:T(8,128)(2,1)S(1)} collective-permute-done((bf16[128,256]{0,1:T(8,128)(2,1)S(1)}, bf16[128,256]{0,1:T(8,128)(2,1)S(1)}, u32[]{:S(2)}, u32[]{:S(2)}) %collective-permute-start.3) | collective-permute-done | bytes 65568 | tf_op jit(solution)/shard_map/ppermute | solution.py:33
  74.7 2.7 collective-permute-start.4
  77.4 4.4 %collective-permute-done.4 = bf16[128,256]{0,1:T(8,128)(2,1)S(1)} collective-permute-done((bf16[128,256]{0,1:T(8,128)(2,1)S(1)}, bf16[128,256]{0,1:T(8,128)(2,1)S(1)}, u32[]{:S(2)}, u32[]{:S(2)}) %collective-permute-start.4) | collective-permute-done | bytes 65568 | tf_op jit(solution)/shard_map/ppermute | solution.py:33
  81.8 8.3 %collective-permute-start.5 = (bf16[128,256]{0,1:T(8,128)(2,1)S(1)}, bf16[128,256]{0,1:T(8,128)(2,1)S(1)}, u32[]{:S(2)}, u32[]{:S(2)}) collective-permute-start(bf16[128,256]{0,1:T(8,128)(2,1)S(1)} %collective-permute-done.4), channel_id=1, source_target_pairs={{0,128},{128,0},{4,132},{132,4},{8,136},{136,8},{12,140},{140,12},... | collective-permute-start | bytes 196616 | tf_op jit(solution)/shard_map/ppermute | solution.py:33
  91.4 2.5 collective-permute-done.5
  93.9 10.0 %collective-permute-start.6 = (bf16[128,256]{0,1:T(8,128)(2,1)S(1)}, bf16[128,256]{0,1:T(8,128)(2,1)S(1)}, u32[]{:S(2)}, u32[]{:S(2)}) collective-permute-start(bf16[128,256]{0,1:T(8,128)(2,1)S(1)} %collective-permute-done.5), channel_id=1, source_target_pairs={{0,256},{256,0},{4,260},{260,4},{8,264},{264,8},{12,268},{268,12},... | collective-permute-start | bytes 196616 | tf_op jit(solution)/shard_map/ppermute | solution.py:33
  104.7 5.9 %collective-permute-done.6 = bf16[128,256]{0,1:T(8,128)(2,1)S(1)} collective-permute-done((bf16[128,256]{0,1:T(8,128)(2,1)S(1)}, bf16[128,256]{0,1:T(8,128)(2,1)S(1)}, u32[]{:S(2)}, u32[]{:S(2)}) %collective-permute-start.6) | collective-permute-done | bytes 65568 | tf_op jit(solution)/shard_map/ppermute | solution.py:33
  110.6 79.4 %all-gather.2.cloned.1.call-done = bf16[32768,128]{0,1:T(8,128)(2,1)} async-done(((bf16[256,128]{0,1:T(8,128)(2,1)}), bf16[32768,128]{0,1:T(8,128)(2,1)}) %all-gather.2.cloned.1.call-update) | async-done | bytes 8388624 | tf_op jit(solution)/shard_map/all_gather | solution.py:99
  190.1 156.1 %while.24 = (s32[]{:T(128)}, f32[1,4,128]{2,1,0:T(4,128)S(1)}, f32[1,4,128]{2,1,0:T(4,128)S(1)}, f32[1,4,128,64]{2,3,1,0:T(8,128)S(1)}, f32[1,4,128]{2,1,0:T(4,1...) while((s32[]{:T(128)}, f32[1,4,128]{2,1,0:T(4,128)S(1)}, ...), condition=%wide.region_11.12_spmd.clone, body=%wide.region_2.11_spmd.clone.sunk | while | flops 278270080 | bytes 14961743 | solution.py:144
  240.6 1.8 conditional.7
  346.2 2.2 collective-permute-start.7
  349.4 1.9 collective-permute-start.8
  351.3 4.2 collective-permute-done.8
  355.5 3.2 collective-permute-start.9
  358.7 4.5 %collective-permute-done.9 = bf16[128,256]{0,1:T(8,128)(2,1)S(1)} collective-permute-done((bf16[128,256]{0,1:T(8,128)(2,1)S(1)}, bf16[128,256]{0,1:T(8,128)(2,1)S(1)}, u32[]{:S(2)}, u32[]{:S(2)}) %collective-permute-start.9) | collective-permute-done | bytes 65568 | tf_op jit(solution)/shard_map/ppermute | solution.py:33
  363.2 2.5 collective-permute-start.10
  365.7 3.6 collective-permute-done.10
  369.3 2.2 collective-permute-start.11
  371.6 4.8 %collective-permute-done.11 = bf16[128,256]{0,1:T(8,128)(2,1)S(1)} collective-permute-done((bf16[128,256]{0,1:T(8,128)(2,1)S(1)}, bf16[128,256]{0,1:T(8,128)(2,1)S(1)}, u32[]{:S(2)}, u32[]{:S(2)}) %collective-permute-start.11) | collective-permute-done | bytes 65568 | tf_op jit(solution)/shard_map/ppermute | solution.py:33
  376.4 4.2 collective-permute-start.12
  380.6 6.5 %collective-permute-done.12 = bf16[128,256]{0,1:T(8,128)(2,1)S(1)} collective-permute-done((bf16[128,256]{0,1:T(8,128)(2,1)S(1)}, bf16[128,256]{0,1:T(8,128)(2,1)S(1)}, u32[]{:S(2)}, u32[]{:S(2)}) %collective-permute-start.12) | collective-permute-done | bytes 65568 | tf_op jit(solution)/shard_map/ppermute | solution.py:33
  387.1 5.7 %collective-permute-start.13 = (bf16[128,256]{0,1:T(8,128)(2,1)S(1)}, bf16[128,256]{0,1:T(8,128)(2,1)S(1)}, u32[]{:S(2)}, u32[]{:S(2)}) collective-permute-start(bf16[128,256]{0,1:T(8,128)(2,1)S(1)} %collective-permute-done.12), channel_id=1, source_target_pairs={{0,256},{256,0},{4,260},{260,4},{8,264},{264,8},{12,268},{268,12},... | collective-permute-start | bytes 196616 | tf_op jit(solution)/shard_map/ppermute | solution.py:33
  392.9 9.1 %collective-permute-done.13 = bf16[128,256]{0,1:T(8,128)(2,1)S(1)} collective-permute-done((bf16[128,256]{0,1:T(8,128)(2,1)S(1)}, bf16[128,256]{0,1:T(8,128)(2,1)S(1)}, u32[]{:S(2)}, u32[]{:S(2)}) %collective-permute-start.13) | collective-permute-done | bytes 65568 | tf_op jit(solution)/shard_map/ppermute | solution.py:33
  402.5 15.0 %all_to_all.16 = bf16[4,64,2048]{2,1,0:T(8,128)(2,1)S(1)} all-to-all(bf16[4,64,2048]{2,1,0:T(8,128)(2,1)S(1)} %bitcast.115), channel_id=1, replica_groups=mesh['sp'=128,'tp'=4] {'tp'}, dimensions={0} | all-to-all | bytes 2097152 | tf_op jit(solution)/shard_map/all_to_all | solution.py:43
  (487 shorter events, 180.1 us)
Async XLA Ops:
  6.5 395.5 %copy-start = (bf16[256,2048]{1,0:T(8,128)(2,1)S(1)}, bf16[256,2048]{1,0:T(8,128)(2,1)}, u32[]{:S(2)}) copy-start(bf16[256,2048]{1,0:T(8,128)(2,1)} %param.16) | copy-start | bytes 3145732
  6.5 20.6 %copy-start.2 = (bf16[2048,64]{0,1:T(8,128)(2,1)S(1)}, bf16[2048,64]{0,1:T(8,128)(2,1)}, u32[]{:S(2)}) copy-start(bf16[2048,64]{0,1:T(8,128)(2,1)} %param.15) | copy-start | bytes 786436
  6.5 183.5 %all-gather.2.cloned.1.call-start = ((), (), s32[]{:S(2)}) async-start(), calls=%async_computation.3 | async-start | bytes 8454144 | tf_op jit(solution)/shard_map/all_gather | solution.py:99
  6.5 21.0 %copy-start.3 = (bf16[2048,64]{0,1:T(8,128)(2,1)S(1)}, bf16[2048,64]{0,1:T(8,128)(2,1)}, u32[]{:S(2)}) copy-start(bf16[2048,64]{0,1:T(8,128)(2,1)} %param.14) | copy-start | bytes 786436
  7.7 20.9 %copy-start.4 = (f32[4,256]{1,0:T(4,128)S(1)}, f32[4,256]{1,0:T(4,128)}, u32[]{:S(2)}) copy-start(f32[4,256]{1,0:T(4,128)} %param.17) | copy-start | bytes 12292
  27.1 21.5 %copy-start.1 = (bf16[2048,256]{1,0:T(8,128)(2,1)S(1)}, bf16[2048,256]{1,0:T(8,128)(2,1)}, u32[]{:S(2)}) copy-start(bf16[2048,256]{1,0:T(8,128)(2,1)} %param.13) | copy-start | bytes 3145732
  29.6 74.4 %all-to-all-start.1 = ((f32[128,4,256]{2,1,0:T(4,128)}), f32[128,4,256]{2,1,0:T(4,128)}, u32[]{:S(2)}, u32[]{:S(2)}) async-start(f32[128,4,256]{2,1,0:T(4,128)} %stack.2), calls=%async_computation.1 | async-start | bytes 1048576 | tf_op jit(solution)/shard_map/all_to_all | solution.py:65
  49.1 3.1 collective-permute-start
  52.3 6.5 %collective-permute-start.1 = (bf16[128,256]{0,1:T(8,128)(2,1)S(1)}, bf16[128,256]{0,1:T(8,128)(2,1)S(1)}, u32[]{:S(2)}, u32[]{:S(2)}) collective-permute-start(bf16[128,256]{0,1:T(8,128)(2,1)S(1)} %collective-permute-done), channel_id=1, source_target_pairs={{0,8},{8,0},{4,12},{12,4},{16,24},{24,16},{20,28},{28,20},{32,40},... | collective-permute-start | bytes 196616 | tf_op jit(solution)/shard_map/ppermute | solution.py:33
  58.7 7.8 %collective-permute-start.2 = (bf16[128,256]{0,1:T(8,128)(2,1)S(1)}, bf16[128,256]{0,1:T(8,128)(2,1)S(1)}, u32[]{:S(2)}, u32[]{:S(2)}) collective-permute-start(bf16[128,256]{0,1:T(8,128)(2,1)S(1)} %collective-permute-done.1), channel_id=1, source_target_pairs={{0,16},{16,0},{4,20},{20,4},{8,24},{24,8},{12,28},{28,12},{32,48},... | collective-permute-start | bytes 196616 | tf_op jit(solution)/shard_map/ppermute | solution.py:33
  66.6 8.1 %collective-permute-start.3 = (bf16[128,256]{0,1:T(8,128)(2,1)S(1)}, bf16[128,256]{0,1:T(8,128)(2,1)S(1)}, u32[]{:S(2)}, u32[]{:S(2)}) collective-permute-start(bf16[128,256]{0,1:T(8,128)(2,1)S(1)} %collective-permute-done.2), channel_id=1, source_target_pairs={{0,32},{32,0},{4,36},{36,4},{8,40},{40,8},{12,44},{44,12},{16,48},... | collective-permute-start | bytes 196616 | tf_op jit(solution)/shard_map/ppermute | solution.py:33
  74.7 7.1 %collective-permute-start.4 = (bf16[128,256]{0,1:T(8,128)(2,1)S(1)}, bf16[128,256]{0,1:T(8,128)(2,1)S(1)}, u32[]{:S(2)}, u32[]{:S(2)}) collective-permute-start(bf16[128,256]{0,1:T(8,128)(2,1)S(1)} %collective-permute-done.3), channel_id=1, source_target_pairs={{0,64},{64,0},{4,68},{68,4},{8,72},{72,8},{12,76},{76,12},{16,80},... | collective-permute-start | bytes 196616 | tf_op jit(solution)/shard_map/ppermute | solution.py:33
  81.8 12.1 %collective-permute-start.5 = (bf16[128,256]{0,1:T(8,128)(2,1)S(1)}, bf16[128,256]{0,1:T(8,128)(2,1)S(1)}, u32[]{:S(2)}, u32[]{:S(2)}) collective-permute-start(bf16[128,256]{0,1:T(8,128)(2,1)S(1)} %collective-permute-done.4), channel_id=1, source_target_pairs={{0,128},{128,0},{4,132},{132,4},{8,136},{136,8},{12,140},{140,12},... | collective-permute-start | bytes 196616 | tf_op jit(solution)/shard_map/ppermute | solution.py:33
  93.9 16.6 %collective-permute-start.6 = (bf16[128,256]{0,1:T(8,128)(2,1)S(1)}, bf16[128,256]{0,1:T(8,128)(2,1)S(1)}, u32[]{:S(2)}, u32[]{:S(2)}) collective-permute-start(bf16[128,256]{0,1:T(8,128)(2,1)S(1)} %collective-permute-done.5), channel_id=1, source_target_pairs={{0,256},{256,0},{4,260},{260,4},{8,264},{264,8},{12,268},{268,12},... | collective-permute-start | bytes 196616 | tf_op jit(solution)/shard_map/ppermute | solution.py:33
  346.2 3.1 collective-permute-start.7
  349.4 6.1 %collective-permute-start.8 = (bf16[128,256]{0,1:T(8,128)(2,1)S(1)}, bf16[128,256]{0,1:T(8,128)(2,1)S(1)}, u32[]{:S(2)}, u32[]{:S(2)}) collective-permute-start(bf16[128,256]{0,1:T(8,128)(2,1)S(1)} %collective-permute-done.7), channel_id=1, source_target_pairs={{0,8},{8,0},{4,12},{12,4},{16,24},{24,16},{20,28},{28,20},{32,40},... | collective-permute-start | bytes 196616 | tf_op jit(solution)/shard_map/ppermute | solution.py:33
  355.5 7.7 %collective-permute-start.9 = (bf16[128,256]{0,1:T(8,128)(2,1)S(1)}, bf16[128,256]{0,1:T(8,128)(2,1)S(1)}, u32[]{:S(2)}, u32[]{:S(2)}) collective-permute-start(bf16[128,256]{0,1:T(8,128)(2,1)S(1)} %collective-permute-done.8), channel_id=1, source_target_pairs={{0,16},{16,0},{4,20},{20,4},{8,24},{24,8},{12,28},{28,12},{32,48},... | collective-permute-start | bytes 196616 | tf_op jit(solution)/shard_map/ppermute | solution.py:33
  363.2 6.1 %collective-permute-start.10 = (bf16[128,256]{0,1:T(8,128)(2,1)S(1)}, bf16[128,256]{0,1:T(8,128)(2,1)S(1)}, u32[]{:S(2)}, u32[]{:S(2)}) collective-permute-start(bf16[128,256]{0,1:T(8,128)(2,1)S(1)} %collective-permute-done.9), channel_id=1, source_target_pairs={{0,32},{32,0},{4,36},{36,4},{8,40},{40,8},{12,44},{44,12},{16,48},... | collective-permute-start | bytes 196616 | tf_op jit(solution)/shard_map/ppermute | solution.py:33
  369.3 7.0 %collective-permute-start.11 = (bf16[128,256]{0,1:T(8,128)(2,1)S(1)}, bf16[128,256]{0,1:T(8,128)(2,1)S(1)}, u32[]{:S(2)}, u32[]{:S(2)}) collective-permute-start(bf16[128,256]{0,1:T(8,128)(2,1)S(1)} %collective-permute-done.10), channel_id=1, source_target_pairs={{0,64},{64,0},{4,68},{68,4},{8,72},{72,8},{12,76},{76,12},{16,80},... | collective-permute-start | bytes 196616 | tf_op jit(solution)/shard_map/ppermute | solution.py:33
  376.4 10.8 %collective-permute-start.12 = (bf16[128,256]{0,1:T(8,128)(2,1)S(1)}, bf16[128,256]{0,1:T(8,128)(2,1)S(1)}, u32[]{:S(2)}, u32[]{:S(2)}) collective-permute-start(bf16[128,256]{0,1:T(8,128)(2,1)S(1)} %collective-permute-done.11), channel_id=1, source_target_pairs={{0,128},{128,0},{4,132},{132,4},{8,136},{136,8},{12,140},{140,12},... | collective-permute-start | bytes 196616 | tf_op jit(solution)/shard_map/ppermute | solution.py:33
  387.1 14.9 %collective-permute-start.13 = (bf16[128,256]{0,1:T(8,128)(2,1)S(1)}, bf16[128,256]{0,1:T(8,128)(2,1)S(1)}, u32[]{:S(2)}, u32[]{:S(2)}) collective-permute-start(bf16[128,256]{0,1:T(8,128)(2,1)S(1)} %collective-permute-done.12), channel_id=1, source_target_pairs={{0,256},{256,0},{4,260},{260,4},{8,264},{264,8},{12,268},{268,12},... | collective-permute-start | bytes 196616 | tf_op jit(solution)/shard_map/ppermute | solution.py:33
Sparse Core Ops, SparseCore 0:
  28.8 161.1 all-gather.1
